TPU v7x, 32 devices: a whole 2x2x4 slice. The times are simulated.
32 devices in a mesh: ep: 8 (over z, core), tp: 4 (over y, x).
Axes of the slice: x: 2, y: 2, z: 4, core: 2. Of those that a mesh axis runs over, the one named last changes fastest.
Arguments:
- tokens: bfloat16 [64, 2048], P('ep'), may hold values from -6 to 6
- attn_gain: float32 [2048], replicated, may hold values from 0.1 to 1.9
- query_weight: bfloat16 [2048, 4096], P('ep', 'tp'), may hold values from -0.125 to 0.125
- key_weight: bfloat16 [2048, 4096], P('ep', 'tp'), may hold values from -0.125 to 0.125
- value_weight: bfloat16 [2048, 4096], P('ep', 'tp'), may hold values from -0.125 to 0.125
- query_gain: float32 [128], replicated, may hold values from 0.1 to 1.9
- stick_bias: float32 [32], P('tp'), may hold values from -7 to -2.5
- key_cache: bfloat16 [64, 32, 512, 128], P('ep', 'tp'), may hold values from -6 to 6
- value_cache: bfloat16 [64, 32, 512, 128], P('ep', 'tp'), may hold values from -6 to 6
- lengths: int32 [64], P('ep'), may hold values from 64 to 512, as said below
- out_weight: bfloat16 [4096, 2048], P('tp'), may hold values from -0.375 to 0.375
- mix_gain: float32 [2048], replicated, may hold values from 0.1 to 1.9
- route_ids: int32 [64, 2], P('ep'), may hold values from 0 to 7, all different within a row; in each aligned block of 8 rows (0 to 7, 8 to 15, ...) at most 4 rows name the same one
- route_weights: float32 [64, 2], P('ep'), may hold values from 0.2 to 1
- expert_gate: bfloat16 [8, 2048, 2560], P('ep', None, 'tp'), may hold values from -0.125 to 0.125
- expert_up: bfloat16 [8, 2048, 2560], P('ep', None, 'tp'), may hold values from -0.125 to 0.125
- expert_down: bfloat16 [8, 2560, 2048], P('ep', 'tp'), may hold values from -0.15625 to 0.15625
- side_gate: bfloat16 [2048, 1024], P(None, 'tp'), may hold values from -0.125 to 0.125
- side_up: bfloat16 [2048, 1024], P(None, 'tp'), may hold values from -0.125 to 0.125
- side_down: bfloat16 [1024, 2048], P('tp'), may hold values from -0.25 to 0.25
- branch_gate: float32 [2048], replicated, may hold values from -0.125 to 0.125
Outputs:
- mixed: bfloat16 [64, 2048], P('ep', 'tp')
- new_keys: bfloat16 [64, 4096], P('ep', 'tp')
- new_values: bfloat16 [64, 4096], P('ep', 'tp')
Inputs may be any that keep to these rules, and one draw needn't show every extreme that they name: `lengths`: at least an eighth of 512; the first sequence has 512. `route_ids`: each token names 2 different experts. In the rows of one device no expert is named by more than 4 rows, a bound that some block reaches of some device.
All inputs are finite; a program needn't handle non-finite values.
Results may differ from a plain program's by a relative error of at most 0.018.
Values may be sent and summed in bfloat16 or wider, within the bound.
No kernel may reach another device: no remote copies, remote signals or barrier semaphores. Data moves between devices by JAX's collectives and lax.ppermute only.
A program may use at most 64 MiB of HBM per device.

v0:
```python
import jax
import jax.numpy as jnp
from jax import lax
from jax.sharding import PartitionSpec as P

DH = 128
epsilon = 1e-06


def rms_scale(values, scale_gain):
    mean_square = jnp.mean(values * values, axis=-1, keepdims=True)
    return values * lax.rsqrt(mean_square + epsilon) * scale_gain


def summed_blocks(partial, axis_name):
    count = lax.axis_size(axis_name)
    rows = partial.shape[0] // count
    blocks = lax.all_to_all(
        partial.astype(jnp.bfloat16), axis_name, split_axis=0, concat_axis=0, tiled=True
    )
    return jnp.sum(blocks.reshape(count, rows, -1).astype(jnp.float32), axis=0)


def body(
    tokens,
    attn_gain,
    query_weight,
    key_weight,
    value_weight,
    query_gain,
    stick_bias,
    key_cache,
    value_cache,
    lengths,
    out_weight,
    mix_gain,
    route_ids,
    route_weights,
    expert_gate,
    expert_up,
    expert_down,
    side_gate,
    side_up,
    side_down,
    branch_gate,
):
    seq_count, model_width = tokens.shape
    head_cols = query_weight.shape[1]
    heads_local = key_cache.shape[1]
    cache_slots = key_cache.shape[2]
    experts = lax.axis_size("ep")
    tp_size = lax.axis_size("tp")
    stream = tokens.astype(jnp.float32)
    normed = rms_scale(stream, attn_gain).astype(jnp.bfloat16)
    columns = lax.all_to_all(normed, "ep", split_axis=1, concat_axis=0, tiled=True)
    query_rows = summed_blocks(
        jnp.dot(columns, query_weight, preferred_element_type=jnp.float32), "ep"
    ).astype(jnp.bfloat16)
    query_heads = rms_scale(
        query_rows.astype(jnp.float32).reshape(seq_count, heads_local, DH), query_gain
    ).astype(jnp.bfloat16)
    fresh = jnp.concatenate(
        [
            jnp.dot(columns, key_weight, preferred_element_type=jnp.float32),
            jnp.dot(columns, value_weight, preferred_element_type=jnp.float32),
        ],
        axis=1,
    )
    fresh = summed_blocks(fresh, "ep").astype(jnp.bfloat16)
    new_values = fresh[:, head_cols:]
    new_keys = rms_scale(
        fresh[:, :head_cols].astype(jnp.float32).reshape(seq_count, heads_local, DH), 1.0
    )
    new_keys = new_keys.astype(jnp.bfloat16).reshape(seq_count, head_cols)
    scores = jnp.einsum("shd,shld->shl", query_heads, key_cache, preferred_element_type=jnp.float32)
    scores = scores * DH ** (-0.5) + stick_bias[None, :, None]
    positions = jnp.arange(cache_slots, dtype=jnp.int32)
    visible = positions[None, None, :] < lengths[:, None, None]
    log_rest = jnp.where(visible, jax.nn.log_sigmoid(-scores), 0.0)
    later = (positions[:, None] > positions[None, :]).astype(jnp.float32)
    log_between = jnp.dot(
        log_rest.reshape(-1, cache_slots), later, precision=lax.Precision.HIGHEST
    ).reshape(scores.shape)
    stick = jnp.where(visible, jnp.exp(jax.nn.log_sigmoid(scores) + log_between), 0.0).astype(
        jnp.bfloat16
    )
    attended = jnp.einsum("shl,shld->shd", stick, value_cache, preferred_element_type=jnp.float32)
    attended = attended.astype(jnp.bfloat16).reshape(seq_count, head_cols)
    attn_part = jnp.dot(attended, out_weight, preferred_element_type=jnp.float32)
    attn_parts = lax.all_gather(attn_part.astype(jnp.bfloat16), "tp", axis=0, tiled=False)
    attn_proj = jnp.sum(attn_parts.astype(jnp.float32), axis=0)
    middle = (stream + attn_proj).astype(jnp.bfloat16)
    normed_mix = rms_scale(middle.astype(jnp.float32), mix_gain).astype(jnp.bfloat16)
    top_count = route_ids.shape[1]
    capacity = max(2, 2 * top_count * seq_count // experts)
    slots = experts * capacity
    flat_ids = route_ids.reshape(-1)
    onehot = (flat_ids[:, None] == jnp.arange(experts, dtype=jnp.int32)[None, :]).astype(jnp.int32)
    order = jnp.arange(flat_ids.shape[0], dtype=jnp.int32)
    earlier = (order[:, None] > order[None, :]) & (flat_ids[:, None] == flat_ids[None, :])
    slot_index = jnp.sum(earlier.astype(jnp.int32), axis=1)
    target = flat_ids * capacity + slot_index
    route_map = (target[:, None] == jnp.arange(slots, dtype=jnp.int32)[None, :]).astype(
        jnp.bfloat16
    )
    dispatch = jnp.sum(route_map.reshape(seq_count, top_count, slots), axis=1).T
    outbox = jnp.dot(dispatch, normed_mix, preferred_element_type=jnp.float32).astype(jnp.bfloat16)
    slot_rows = lax.all_to_all(outbox, "ep", split_axis=0, concat_axis=0, tiled=True)
    side_gate_pre = jnp.dot(normed_mix, side_gate, preferred_element_type=jnp.float32)
    side_up_pre = jnp.dot(normed_mix, side_up, preferred_element_type=jnp.float32)
    side_hidden = (jax.nn.silu(side_gate_pre) * side_up_pre).astype(jnp.bfloat16)
    side_term = jnp.dot(side_hidden, side_down, preferred_element_type=jnp.float32)
    switch = jax.nn.sigmoid(
        jnp.sum(normed_mix.astype(jnp.float32) * branch_gate, axis=1, keepdims=True)
    )
    col_width = model_width // tp_size
    col_offset = lax.axis_index("tp") * col_width
    side_blocks = lax.all_to_all(
        side_term.astype(jnp.bfloat16).reshape(seq_count, tp_size, col_width).transpose(1, 0, 2),
        "tp",
        split_axis=0,
        concat_axis=0,
        tiled=True,
    )
    side_part = jnp.sum(side_blocks.astype(jnp.float32), axis=0)
    gate_pre = jnp.dot(slot_rows, expert_gate[0], preferred_element_type=jnp.float32)
    up_pre = jnp.dot(slot_rows, expert_up[0], preferred_element_type=jnp.float32)
    hidden = (jax.nn.silu(gate_pre) * up_pre).astype(jnp.bfloat16)
    expert_term = jnp.dot(hidden, expert_down[0], preferred_element_type=jnp.float32)
    expert_term = expert_term.astype(jnp.bfloat16).reshape(experts, capacity, tp_size, col_width)
    returned = lax.all_to_all(
        expert_term.transpose(0, 2, 1, 3).reshape(experts * tp_size, capacity, col_width),
        ("ep", "tp"),
        split_axis=0,
        concat_axis=0,
        tiled=True,
    )
    expert_out = jnp.sum(
        returned.reshape(experts, tp_size, capacity, col_width).astype(jnp.float32), axis=1
    ).astype(jnp.bfloat16)
    picked = jnp.dot(
        route_map, expert_out.reshape(slots, col_width), preferred_element_type=jnp.float32
    )
    routed = jnp.sum(
        route_weights[:, :, None] * picked.reshape(seq_count, top_count, col_width), axis=1
    )
    middle_cols = lax.dynamic_slice_in_dim(middle, col_offset, col_width, 1).astype(jnp.float32)
    mixed = (middle_cols + routed + switch * side_part).astype(jnp.bfloat16)
    return (mixed, new_keys, new_values)


def solution(mesh):
    in_specs = (
        P("ep", None),
        P(),
        P("ep", "tp"),
        P("ep", "tp"),
        P("ep", "tp"),
        P(),
        P("tp"),
        P("ep", "tp", None, None),
        P("ep", "tp", None, None),
        P("ep"),
        P("tp", None),
        P(),
        P("ep", None),
        P("ep", None),
        P("ep", None, "tp"),
        P("ep", None, "tp"),
        P("ep", "tp", None),
        P(None, "tp"),
        P(None, "tp"),
        P("tp", None),
        P(),
    )
    out_specs = (P("ep", "tp"), P("ep", "tp"), P("ep", "tp"))
    return jax.shard_map(body, mesh=mesh, in_specs=in_specs, out_specs=out_specs, check_vma=False)
```

profile of v0, /device:TPU:0, one launch (start us, length us, event | category | flops | bytes accessed | tf_op | source)
XLA Modules:
  0.0 91.9 jit_solution(14223555700688407675)
XLA Ops:
  0.7 1.0 %fusion.50 = f32[8]{0:T(128)S(1)} fusion(bf16[8,2048]{1,0:T(8,128)(2,1)} %param.21), kind=kLoop, calls=%fused_computation.61 | loop fusion | flops 49144 | bytes 32800 | tf_op jit(solution)/shard_map/reduce_sum | solution.py:11
  1.7 1.4 %fusion.52 = bf16[8,2048]{1,0:T(8,128)(2,1)} fusion(bf16[8,2048]{1,0:T(8,128)(2,1)} %param.21, f32[2048]{0:T(1024)} %param.22, f32[8]{0:T(128)S(1)} %add_rsqrt_fusion.3), kind=kLoop, calls=%fused_computation.63 | loop fusion | flops 65536 | bytes 73760 | tf_op jit(solution)/shard_map/convert_element_type | solution.py:54
  3.2 6.4 %all-to-all-start = ((bf16[8,8,256]{2,0,1:T(8,128)(2,1)}), bf16[8,8,256]{2,0,1:T(8,128)(2,1)S(1)}, u32[]{:S(2)}, u32[]{:S(2)}) async-start(bf16[8,8,256]{2,0,1:T(8,128)(2,1)} %bitcast), calls=%async_computation | async-start | bytes 65536 | tf_op jit(solution)/shard_map/all_to_all | solution.py:55
  9.5 0.7 iota_compare_fusion.1
  10.2 0.8 copy.31
  11.0 0.1 eq.51
  11.1 0.2 convert_reduce_fusion.2
  11.3 0.1 reduce_sum.136
  11.3 0.1 copy.33
  11.4 0.1 fusion.82
  11.5 3.7 %all-to-all-done = bf16[8,8,256]{2,0,1:T(8,128)(2,1)S(1)} async-done(((bf16[8,8,256]{2,0,1:T(8,128)(2,1)}), bf16[8,8,256]{2,0,1:T(8,128)(2,1)S(1)}, u32[]{:S(2)}, u32[]{:S(2)}) %all-to-all-start) | async-done | bytes 32800 | tf_op jit(solution)/shard_map/all_to_all | solution.py:55
  15.2 1.9 %fusion.9 = bf16[8,8,1024]{2,1,0:T(8,128)(2,1)} fusion(bf16[256,1024]{1,0:T(8,128)(2,1)} %param.23, bf16[8,8,256]{2,0,1:T(8,128)(2,1)S(1)} %all-to-all-done), kind=kOutput, calls=%fused_computation.13 | convolution fusion | flops 33619968 | bytes 688128 | tf_op jit(solution)/shard_map/dot_general | solution.py:57
  17.2 3.4 %all-to-all-start.1 = ((bf16[8,8,1024]{2,1,0:T(8,128)(2,1)}), bf16[8,8,1024]{2,1,0:T(8,128)(2,1)S(1)}, u32[]{:S(2)}, u32[]{:S(2)}) async-start(bf16[8,8,1024]{2,1,0:T(8,128)(2,1)} %fusion.9), calls=%async_computation.1 | async-start | bytes 262144 | tf_op jit(solution)/shard_map/all_to_all | solution.py:18
  20.5 1.3 %convolution_convert_fusion.3 = bf16[8,8,1024]{2,1,0:T(8,128)(2,1)S(1)} fusion(bf16[256,1024]{1,0:T(8,128)(2,1)} %param.25, bf16[8,8,256]{2,0,1:T(8,128)(2,1)S(1)} %all-to-all-done), kind=kOutput, calls=%fused_computation.10 | convolution fusion | flops 33619968 | bytes 688128 | tf_op jit(solution)/shard_map/dot_general | solution.py:65
  21.8 1.3 %convolution_convert_fusion.4 = bf16[8,8,1024]{2,1,0:T(8,128)(2,1)S(1)} fusion(bf16[256,1024]{1,0:T(8,128)(2,1)} %param.24, bf16[8,8,256]{2,0,1:T(8,128)(2,1)S(1)} %all-to-all-done), kind=kOutput, calls=%fused_computation.11 | convolution fusion | flops 33619968 | bytes 688128 | tf_op jit(solution)/shard_map/dot_general | solution.py:64
  23.1 0.7 pad_maximum_fusion
  23.8 3.5 %all-to-all-done.1 = bf16[8,8,1024]{2,1,0:T(8,128)(2,1)S(1)} async-done(((bf16[8,8,1024]{2,1,0:T(8,128)(2,1)}), bf16[8,8,1024]{2,1,0:T(8,128)(2,1)S(1)}, u32[]{:S(2)}, u32[]{:S(2)}) %all-to-all-start.1) | async-done | bytes 131104 | tf_op jit(solution)/shard_map/all_to_all | solution.py:18
  27.2 0.1 fusion.62
  27.3 0.1 fusion.70
  27.4 5.8 %fusion.68 = f32[8,8,1,512]{3,2,1,0:T(1,128)S(1)} fusion(bf16[8,8,512,128]{3,2,1,0:T(8,128)(2,1)} %param.28, bf16[8,8,128,1]{2,0,1,3:T(8,128)(2,1)S(1)} %fusion.70), kind=kOutput, calls=%fused_computation.85 | convolution fusion | flops 8388608 | bytes 8536064 | tf_op jit(solution)/shard_map/shd,shld->shl/dot_general | solution.py:75
  33.2 0.6 fusion.16
  33.8 1.2 %fusion.33 = f32[8,8,1,128]{3,2,1,0:T(1,128)S(1)} fusion(bf16[8,8,512,128]{3,2,1,0:T(8,128)(2,1)S(1)} %copy-done.1, bf16[8,8,512,1]{2,1,0,3:T(8,128)(2,1)S(1)} %fusion.16), kind=kOutput, calls=%fused_computation.39 | convolution fusion | flops 8388608 | bytes 8486912 | tf_op jit(solution)/shard_map/shl,shld->shd/dot_general | solution.py:87
  35.0 1.0 %copy-done.2 = bf16[1024,2048]{1,0:T(8,128)(2,1)S(1)} copy-done((bf16[1024,2048]{1,0:T(8,128)(2,1)S(1)}, bf16[1024,2048]{1,0:T(8,128)(2,1)}, u32[]{:S(2)}) %copy-start.2) | copy-done | bytes 4194328
  36.0 0.7 convolution_convert_fusion.2
  36.7 8.6 %all-gather = bf16[32,2048]{1,0:T(8,128)(2,1)S(1)} all-gather(bf16[8,2048]{1,0:T(8,128)(2,1)S(1)} %convolution_convert_fusion.2), channel_id=2, replica_groups=mesh['ep'=8,'tp'=4] {'tp'}, dimensions={0}, use_global_device_ids=true | all-gather | bytes 163840 | tf_op jit(solution)/shard_map/all_gather | solution.py:90
  45.3 0.1 fusion.47
  45.4 0.2 convolution_convert_fusion
  45.7 0.3 fusion.91
  46.0 2.9 %convolution_convert_fusion.1 = bf16[8,2048]{1,0:T(8,128)(2,1)} fusion(bf16[256,2048]{1,0:T(8,128)(2,1)} %param.40, bf16[2048,256]{1,0:T(8,128)(2,1)} %param.39, f32[8,256]{1,0:T(8,128)S(1)} %fusion.91, bf16[8,2048]{1,0:T(8,128)(2,1)S(1)} %get-tuple-element.4, f32[2048]{0:T(1024)S(1)} %copy-done.5, f32[8]{0:T(128)S(1)} %add_rsqrt_fusion.2), kind=kOutput, calls=%fused_computation.8 | convolution fusion | flops 16871424 | bytes 2179104 | tf_op jit(solution)/shard_map/dot_general | solution.py:112
  48.9 3.3 %all-to-all-start.4 = ((bf16[4,8,512]{2,1,0:T(8,128)(2,1)}), bf16[4,8,512]{2,1,0:T(8,128)(2,1)S(1)}, u32[]{:S(2)}, u32[]{:S(2)}) async-start(bf16[4,8,512]{2,1,0:T(8,128)(2,1)} %bitcast.21), calls=%async_computation.4 | async-start | bytes 65536 | tf_op jit(solution)/shard_map/all_to_all | solution.py:118
  52.2 0.2 multiply_reduce_fusion
  52.4 0.7 all_to_all.44
  53.1 3.8 %all-to-all-done.4 = bf16[4,8,512]{2,1,0:T(8,128)(2,1)S(1)} async-done(((bf16[4,8,512]{2,1,0:T(8,128)(2,1)}), bf16[4,8,512]{2,1,0:T(8,128)(2,1)S(1)}, u32[]{:S(2)}, u32[]{:S(2)}) %all-to-all-start.4) | async-done | bytes 32800 | tf_op jit(solution)/shard_map/all_to_all | solution.py:118
  56.9 3.4 %all-to-all-start.2 = ((bf16[8,4,2048]{2,1,0:T(4,128)(2,1)}), bf16[8,4,2048]{2,1,0:T(4,128)(2,1)S(1)}, u32[]{:S(2)}, u32[]{:S(2)}) async-start(bf16[8,4,2048]{2,1,0:T(4,128)(2,1)} %all_to_all.44), calls=%async_computation.2 | async-start | bytes 262144 | tf_op jit(solution)/shard_map/all_to_all | solution.py:108
  60.3 6.7 %all-to-all-done.2 = bf16[8,4,2048]{2,1,0:T(4,128)(2,1)S(1)} async-done(((bf16[8,4,2048]{2,1,0:T(4,128)(2,1)}), bf16[8,4,2048]{2,1,0:T(4,128)(2,1)S(1)}, u32[]{:S(2)}, u32[]{:S(2)}) %all-to-all-start.2) | async-done | bytes 131104 | tf_op jit(solution)/shard_map/all_to_all | solution.py:108
  66.9 3.4 %all-to-all-start.5 = ((bf16[8,8,2048]{2,1,0:T(8,128)(2,1)}), bf16[8,8,2048]{2,1,0:T(8,128)(2,1)S(1)}, u32[]{:S(2)}, u32[]{:S(2)}) async-start(bf16[8,8,2048]{2,1,0:T(8,128)(2,1)} %pad_maximum_fusion), calls=%async_computation.5 | async-start | bytes 524288 | tf_op jit(solution)/shard_map/all_to_all | solution.py:18
  70.4 2.3 %fusion.4 = f32[32,640]{1,0:T(8,128)S(1)} fusion(bf16[32,2048]{1,0:T(8,128)(2,1)S(1)} %all_to_all.46, bf16[1,2048,640]{2,1,0:T(8,128)(2,1)} %param.35), kind=kOutput, calls=%fused_computation.4 | convolution fusion | flops 83886080 | bytes 2834432 | tf_op jit(solution)/shard_map/dot_general | solution.py:126
  72.7 2.7 %fusion.6 = bf16[32,2048]{1,0:T(8,128)(2,1)S(1)} fusion(bf16[1,640,2048]{2,1,0:T(8,128)(2,1)S(1)} %copy-done, bf16[32,2048]{1,0:T(8,128)(2,1)S(1)} %all_to_all.46, bf16[1,2048,640]{2,1,0:T(8,128)(2,1)} %param.36, f32[32,640]{1,0:T(8,128)S(1)} %fusion.4), kind=kOutput, calls=%fused_computation.6 | convolution fusion | flops 167960576 | bytes 5586944 | tf_op jit(solution)/shard_map/dot_general | solution.py:129
  75.4 0.1 reshape.169
  75.5 0.7 copy.35
  76.2 3.8 %all-to-all-done.5 = bf16[8,8,2048]{2,1,0:T(8,128)(2,1)S(1)} async-done(((bf16[8,8,2048]{2,1,0:T(8,128)(2,1)}), bf16[8,8,2048]{2,1,0:T(8,128)(2,1)S(1)}, u32[]{:S(2)}, u32[]{:S(2)}) %all-to-all-start.5) | async-done | bytes 262176 | tf_op jit(solution)/shard_map/all_to_all | solution.py:18
  80.0 2.6 %all-to-all-start.3 = ((bf16[32,4,512]{2,1,0:T(4,128)(2,1)}), bf16[32,4,512]{2,1,0:T(4,128)(2,1)S(1)}, u32[]{:S(2)}, u32[]{:S(2)}) async-start(bf16[32,4,512]{2,1,0:T(4,128)(2,1)} %bitcast.18), calls=%async_computation.3 | async-start | bytes 262144 | tf_op jit(solution)/shard_map/all_to_all | solution.py:131
  82.6 0.1 fusion.60
  82.7 0.6 slice.9
  83.3 0.7 fusion.61
  84.0 6.9 %all-to-all-done.3 = bf16[32,4,512]{2,1,0:T(4,128)(2,1)S(1)} async-done(((bf16[32,4,512]{2,1,0:T(4,128)(2,1)}), bf16[32,4,512]{2,1,0:T(4,128)(2,1)S(1)}, u32[]{:S(2)}, u32[]{:S(2)}) %all-to-all-start.3) | async-done | bytes 131104 | tf_op jit(solution)/shard_map/all_to_all | solution.py:131
  91.0 0.2 fusion.20
  91.2 0.7 add_convert_fusion
  (33 shorter events, 0.3 us)
Async XLA Ops:
  0.6 72.0 %copy-start = (bf16[1,640,2048]{2,1,0:T(8,128)(2,1)S(1)}, bf16[1,640,2048]{2,1,0:T(8,128)(2,1)}, u32[]{:S(2)}) copy-start(bf16[1,640,2048]{2,1,0:T(8,128)(2,1)} %param.37) | copy-start | bytes 7864324
  0.6 26.7 %copy-start.7 = (f32[128]{0:T(128)S(1)}, f32[128]{0:T(128)}, u32[]{:S(2)}) copy-start(f32[128]{0:T(128)} %param.26) | copy-start | bytes 1540
  3.2 12.1 %all-to-all-start = ((bf16[8,8,256]{2,0,1:T(8,128)(2,1)}), bf16[8,8,256]{2,0,1:T(8,128)(2,1)S(1)}, u32[]{:S(2)}, u32[]{:S(2)}) async-start(bf16[8,8,256]{2,0,1:T(8,128)(2,1)} %bitcast), calls=%async_computation | async-start | bytes 65536 | tf_op jit(solution)/shard_map/all_to_all | solution.py:55
  17.2 10.1 %all-to-all-start.1 = ((bf16[8,8,1024]{2,1,0:T(8,128)(2,1)}), bf16[8,8,1024]{2,1,0:T(8,128)(2,1)S(1)}, u32[]{:S(2)}, u32[]{:S(2)}) async-start(bf16[8,8,1024]{2,1,0:T(8,128)(2,1)} %fusion.9), calls=%async_computation.1 | async-start | bytes 262144 | tf_op jit(solution)/shard_map/all_to_all | solution.py:18
  27.4 5.8 %copy-start.9 = (f32[8]{0:T(128)S(1)}, f32[8]{0:T(128)}, u32[]{:S(2)}) copy-start(f32[8]{0:T(128)} %param.27) | copy-start | bytes 100
  27.4 6.4 %copy-start.1 = (bf16[8,8,512,128]{3,2,1,0:T(8,128)(2,1)S(1)}, bf16[8,8,512,128]{3,2,1,0:T(8,128)(2,1)}, u32[]{:S(2)}) copy-start(bf16[8,8,512,128]{3,2,1,0:T(8,128)(2,1)} %param.29) | copy-start | bytes 25165828
  33.8 2.2 %copy-start.2 = (bf16[1024,2048]{1,0:T(8,128)(2,1)S(1)}, bf16[1024,2048]{1,0:T(8,128)(2,1)}, u32[]{:S(2)}) copy-start(bf16[1024,2048]{1,0:T(8,128)(2,1)} %param.31) | copy-start | bytes 12582916
  35.0 10.3 %copy-start.4 = (bf16[8,2048]{1,0:T(8,128)(2,1)S(1)}, bf16[8,2048]{1,0:T(8,128)(2,1)}, u32[]{:S(2)}) copy-start(bf16[8,2048]{1,0:T(8,128)(2,1)} %param.21) | copy-start | bytes 98308
  35.0 10.4 %copy-start.5 = (f32[2048]{0:T(1024)S(1)}, f32[2048]{0:T(1024)}, u32[]{:S(2)}) copy-start(f32[2048]{0:T(1024)} %param.32) | copy-start | bytes 24580
  35.0 10.7 %copy-start.3 = (bf16[2048,256]{1,0:T(8,128)(2,1)S(1)}, bf16[2048,256]{1,0:T(8,128)(2,1)}, u32[]{:S(2)}) copy-start(bf16[2048,256]{1,0:T(8,128)(2,1)} %param.38) | copy-start | bytes 3145732
  36.7 15.5 %copy-start.6 = (f32[2048]{0:T(1024)S(1)}, f32[2048]{0:T(1024)}, u32[]{:S(2)}) copy-start(f32[2048]{0:T(1024)} %param.41) | copy-start | bytes 24580
  48.9 8.0 %all-to-all-start.4 = ((bf16[4,8,512]{2,1,0:T(8,128)(2,1)}), bf16[4,8,512]{2,1,0:T(8,128)(2,1)S(1)}, u32[]{:S(2)}, u32[]{:S(2)}) async-start(bf16[4,8,512]{2,1,0:T(8,128)(2,1)} %bitcast.21), calls=%async_computation.4 | async-start | bytes 65536 | tf_op jit(solution)/shard_map/all_to_all | solution.py:118
  56.9 10.1 %all-to-all-start.2 = ((bf16[8,4,2048]{2,1,0:T(4,128)(2,1)}), bf16[8,4,2048]{2,1,0:T(4,128)(2,1)S(1)}, u32[]{:S(2)}, u32[]{:S(2)}) async-start(bf16[8,4,2048]{2,1,0:T(4,128)(2,1)} %all_to_all.44), calls=%async_computation.2 | async-start | bytes 262144 | tf_op jit(solution)/shard_map/all_to_all | solution.py:108
  66.9 13.1 %all-to-all-start.5 = ((bf16[8,8,2048]{2,1,0:T(8,128)(2,1)}), bf16[8,8,2048]{2,1,0:T(8,128)(2,1)S(1)}, u32[]{:S(2)}, u32[]{:S(2)}) async-start(bf16[8,8,2048]{2,1,0:T(8,128)(2,1)} %pad_maximum_fusion), calls=%async_computation.5 | async-start | bytes 524288 | tf_op jit(solution)/shard_map/all_to_all | solution.py:18
  72.7 18.4 %copy-start.8 = (f32[8,2]{0,1:T(2,128)S(1)}, f32[8,2]{0,1:T(2,128)}, u32[]{:S(2)}) copy-start(f32[8,2]{0,1:T(2,128)} %param.34) | copy-start | bytes 196
  80.0 10.9 %all-to-all-start.3 = ((bf16[32,4,512]{2,1,0:T(4,128)(2,1)}), bf16[32,4,512]{2,1,0:T(4,128)(2,1)S(1)}, u32[]{:S(2)}, u32[]{:S(2)}) async-start(bf16[32,4,512]{2,1,0:T(4,128)(2,1)} %bitcast.18), calls=%async_computation.3 | async-start | bytes 262144 | tf_op jit(solution)/shard_map/all_to_all | solution.py:131
where the time goes:
time: 92.9 us; the launch traced here: 91.9 us
  waiting for transfers between devices  28.4 us (31%)
  starting transfers between devices  22.3 us (24%)
  matrix products  21.2 us (23%)
  blocking collectives  8.59 us (9%)
  other arithmetic  6.32 us (7%)
  local copies, waits for them, and re-layouts  4.18 us (4%)
    all_gather x1, blocking collectives, body(): lax.all_gather(attn_part.astype(jnp.bfloat16), 'tp', axis=0, tiled=False)  8.59 us
    all_to_all x2, waiting for transfers between devices, summed_blocks(): lax.all_to_all(partial.astype(jnp.bfloat16), axis_name, split_axis=0, con...  7.22 us
    all_to_all x1, waiting for transfers between devices, body(): lax.all_to_all(expert_term.transpose(0, 2, 1, 3).reshape(experts * tp_siz...  6.94 us
    all_to_all x2, starting transfers between devices, summed_blocks(): lax.all_to_all(partial.astype(jnp.bfloat16), axis_name, split_axis=0, con...  6.78 us
    all_to_all x1, waiting for transfers between devices, body(): lax.all_to_all(outbox, 'ep', split_axis=0, concat_axis=0, tiled=True)  6.65 us
    all_to_all x1, starting transfers between devices, body(): lax.all_to_all(normed, 'ep', split_axis=1, concat_axis=0, tiled=True)  6.35 us
    dot_general x1, matrix products, body(): jnp.einsum('shd,shld->shl', query_heads, key_cache, preferred_element_typ...  5.79 us
    all_to_all x1, waiting for transfers between devices, body(): lax.all_to_all(side_term.astype(jnp.bfloat16).reshape(seq_count, tp_size,...  3.8 us
  transfers between devices with their start and end apart: 6, of which 6 were waited for; matrix products, arithmetic and copies ran while one was open for 14% of the time, Pallas kernels for 0%

commit v1 on v0

--- a/solution.py
+++ b/solution.py
@@ -5,6 +5,12 @@
 
 DH = 128
 epsilon = 1e-06
+
+
+def stacked_exchange(array, name, split, join):
+    pieces = jnp.split(array, lax.axis_size(name), axis=split)
+    received = lax.all_to_all(jnp.stack(pieces), name, 0, 0)
+    return jnp.concatenate(received, axis=join)
 
 
 def rms_scale(values, scale_gain):
@@ -52,7 +58,7 @@
     tp_size = lax.axis_size("tp")
     stream = tokens.astype(jnp.float32)
     normed = rms_scale(stream, attn_gain).astype(jnp.bfloat16)
-    columns = lax.all_to_all(normed, "ep", split_axis=1, concat_axis=0, tiled=True)
+    columns = stacked_exchange(normed, "ep", 1, 0)
     query_rows = summed_blocks(
         jnp.dot(columns, query_weight, preferred_element_type=jnp.float32), "ep"
     ).astype(jnp.bfloat16)

time: 92.9 us -> 96.8 us (1.042)
  local copies, waits for them, and re-layouts: 4.18 us -> 8.91 us
    unnamed x21 -> x28, local copies, waits for them, and re-layouts: 1.76 us -> 5.9 us
  transfers between devices with their start and end apart: 6 -> 6, of which waited for: 6 -> 6; matrix products, arithmetic and copies ran while one was open for 14% -> 13% of each run, Pallas kernels for 0% -> 0%
where the time goes in v1:
time: 96.8 us; the launch traced here: 95.8 us
  waiting for transfers between devices  28.1 us (29%)
  starting transfers between devices  22.3 us (23%)
  matrix products  21.2 us (22%)
  local copies, waits for them, and re-layouts  8.91 us (9%)
  blocking collectives  8.59 us (9%)
  other arithmetic  5.72 us (6%)
    all_gather x1, blocking collectives, body(): lax.all_gather(attn_part.astype(jnp.bfloat16), 'tp', axis=0, tiled=False)  8.59 us
    all_to_all x2, waiting for transfers between devices, summed_blocks(): lax.all_to_all(partial.astype(jnp.bfloat16), axis_name, split_axis=0, con...  7.22 us
    all_to_all x1, waiting for transfers between devices, body(): lax.all_to_all(expert_term.transpose(0, 2, 1, 3).reshape(experts * tp_siz...  6.94 us
    all_to_all x2, starting transfers between devices, summed_blocks(): lax.all_to_all(partial.astype(jnp.bfloat16), axis_name, split_axis=0, con...  6.78 us
    all_to_all x1, waiting for transfers between devices, body(): lax.all_to_all(outbox, 'ep', split_axis=0, concat_axis=0, tiled=True)  6.65 us
    all_to_all x1, starting transfers between devices, stacked_exchange(): received = lax.all_to_all(jnp.stack(pieces), name, 0, 0)  6.35 us
    unnamed x28, local copies, waits for them, and re-layouts  5.9 us
    dot_general x1, matrix products, body(): jnp.einsum('shd,shld->shl', query_heads, key_cache, preferred_element_typ...  5.79 us
  transfers between devices with their start and end apart: 6, of which 6 were waited for; matrix products, arithmetic and copies ran while one was open for 13% of the time, Pallas kernels for 0%

profile of v1, /device:TPU:0, one launch (start us, length us, event | category | flops | bytes accessed | tf_op | source)
XLA Modules:
  0.0 95.8 jit_solution(17144845823048908760)
XLA Ops:
  0.7 1.0 %fusion.50 = f32[8]{0:T(128)S(1)} fusion(bf16[8,2048]{1,0:T(8,128)(2,1)} %param.21), kind=kLoop, calls=%fused_computation.61 | loop fusion | flops 49144 | bytes 32800 | tf_op jit(solution)/shard_map/reduce_sum | solution.py:17
  1.7 0.8 fusion.52
  2.6 0.6 constant_dynamic-update-slice_fusion.7
  3.1 0.6 constant_dynamic-update-slice_fusion.6
  3.7 0.6 constant_dynamic-update-slice_fusion.5
  4.3 0.6 constant_dynamic-update-slice_fusion.4
  4.9 0.6 constant_dynamic-update-slice_fusion.3
  5.5 0.6 constant_dynamic-update-slice_fusion.2
  6.1 0.6 constant_dynamic-update-slice_fusion.1
  6.7 0.6 constant_dynamic-update-slice_fusion
  7.3 6.4 %all-to-all-start = ((bf16[8,8,256]{2,1,0:T(8,128)(2,1)}), bf16[8,8,256]{2,1,0:T(8,128)(2,1)S(1)}, u32[]{:S(2)}, u32[]{:S(2)}) async-start(bf16[8,8,256]{2,1,0:T(8,128)(2,1)} %constant_dynamic-update-slice_fusion), calls=%async_computation | async-start | bytes 65536 | tf_op jit(solution)/shard_map/all_to_all | solution.py:12
  13.6 0.7 iota_compare_fusion.1
  14.4 0.8 copy.31
  15.2 0.2 convert_reduce_fusion.2
  15.6 3.7 %all-to-all-done = bf16[8,8,256]{2,1,0:T(8,128)(2,1)S(1)} async-done(((bf16[8,8,256]{2,1,0:T(8,128)(2,1)}), bf16[8,8,256]{2,1,0:T(8,128)(2,1)S(1)}, u32[]{:S(2)}, u32[]{:S(2)}) %all-to-all-start) | async-done | bytes 32800 | tf_op jit(solution)/shard_map/all_to_all | solution.py:12
  19.4 1.9 %fusion.9 = bf16[8,8,1024]{2,1,0:T(8,128)(2,1)} fusion(bf16[256,1024]{1,0:T(8,128)(2,1)} %param.23, bf16[8,8,256]{2,1,0:T(8,128)(2,1)S(1)} %all-to-all-done), kind=kOutput, calls=%fused_computation.13 | convolution fusion | flops 33619968 | bytes 688128 | tf_op jit(solution)/shard_map/dot_general | solution.py:63
  21.3 3.4 %all-to-all-start.1 = ((bf16[8,8,1024]{2,1,0:T(8,128)(2,1)}), bf16[8,8,1024]{2,1,0:T(8,128)(2,1)S(1)}, u32[]{:S(2)}, u32[]{:S(2)}) async-start(bf16[8,8,1024]{2,1,0:T(8,128)(2,1)} %fusion.9), calls=%async_computation.1 | async-start | bytes 262144 | tf_op jit(solution)/shard_map/all_to_all | solution.py:24
  24.7 1.3 %convolution_convert_fusion.3 = bf16[8,8,1024]{2,1,0:T(8,128)(2,1)S(1)} fusion(bf16[8,8,256]{2,1,0:T(8,128)(2,1)S(1)} %all-to-all-done, bf16[256,1024]{1,0:T(8,128)(2,1)} %param.25), kind=kOutput, calls=%fused_computation.10 | convolution fusion | flops 33619968 | bytes 688128 | tf_op jit(solution)/shard_map/dot_general | solution.py:71
  25.9 1.3 %convolution_convert_fusion.4 = bf16[8,8,1024]{2,1,0:T(8,128)(2,1)S(1)} fusion(bf16[8,8,256]{2,1,0:T(8,128)(2,1)S(1)} %all-to-all-done, bf16[256,1024]{1,0:T(8,128)(2,1)} %param.24), kind=kOutput, calls=%fused_computation.11 | convolution fusion | flops 33619968 | bytes 688128 | tf_op jit(solution)/shard_map/dot_general | solution.py:70
  27.2 0.7 pad_maximum_fusion
  27.9 3.5 %all-to-all-done.1 = bf16[8,8,1024]{2,1,0:T(8,128)(2,1)S(1)} async-done(((bf16[8,8,1024]{2,1,0:T(8,128)(2,1)}), bf16[8,8,1024]{2,1,0:T(8,128)(2,1)S(1)}, u32[]{:S(2)}, u32[]{:S(2)}) %all-to-all-start.1) | async-done | bytes 131104 | tf_op jit(solution)/shard_map/all_to_all | solution.py:24
  31.6 5.8 %fusion.66 = f32[8,8,1,512]{3,2,1,0:T(1,128)S(1)} fusion(bf16[8,8,512,128]{3,2,1,0:T(8,128)(2,1)} %param.28, bf16[8,8,128,1]{2,0,1,3:T(8,128)(2,1)S(1)} %fusion.68), kind=kOutput, calls=%fused_computation.83 | convolution fusion | flops 8388608 | bytes 8536064 | tf_op jit(solution)/shard_map/shd,shld->shl/dot_general | solution.py:81
  37.4 0.6 fusion.16
  38.0 1.2 %fusion.33 = f32[8,8,1,128]{3,2,1,0:T(1,128)S(1)} fusion(bf16[8,8,512,128]{3,2,1,0:T(8,128)(2,1)S(1)} %copy-done.1, bf16[8,8,512,1]{2,1,0,3:T(8,128)(2,1)S(1)} %fusion.16), kind=kOutput, calls=%fused_computation.39 | convolution fusion | flops 8388608 | bytes 8486912 | tf_op jit(solution)/shard_map/shl,shld->shd/dot_general | solution.py:93
  39.2 1.0 %copy-done.2 = bf16[1024,2048]{1,0:T(8,128)(2,1)S(1)} copy-done((bf16[1024,2048]{1,0:T(8,128)(2,1)S(1)}, bf16[1024,2048]{1,0:T(8,128)(2,1)}, u32[]{:S(2)}) %copy-start.2) | copy-done | bytes 4194328
  40.1 0.7 convolution_convert_fusion.2
  40.8 8.6 %all-gather = bf16[32,2048]{1,0:T(8,128)(2,1)S(1)} all-gather(bf16[8,2048]{1,0:T(8,128)(2,1)S(1)} %convolution_convert_fusion.2), channel_id=2, replica_groups=mesh['ep'=8,'tp'=4] {'tp'}, dimensions={0}, use_global_device_ids=true | all-gather | bytes 163840 | tf_op jit(solution)/shard_map/all_gather | solution.py:96
  49.4 0.1 fusion.47
  49.6 0.3 fusion.89
  49.9 2.9 %convolution_convert_fusion.1 = bf16[8,2048]{1,0:T(8,128)(2,1)} fusion(bf16[256,2048]{1,0:T(8,128)(2,1)} %param.40, bf16[2048,256]{1,0:T(8,128)(2,1)} %param.39, f32[8,256]{1,0:T(8,128)S(1)} %fusion.89, bf16[8,2048]{1,0:T(8,128)(2,1)S(1)} %get-tuple-element.4, f32[2048]{0:T(1024)S(1)} %copy-done.5, f32[8]{0:T(128)S(1)} %add_rsqrt_fusion.2), kind=kOutput, calls=%fused_computation.8 | convolution fusion | flops 16871424 | bytes 2179104 | tf_op jit(solution)/shard_map/dot_general | solution.py:118
  52.8 3.3 %all-to-all-start.4 = ((bf16[4,8,512]{2,1,0:T(8,128)(2,1)}), bf16[4,8,512]{2,1,0:T(8,128)(2,1)S(1)}, u32[]{:S(2)}, u32[]{:S(2)}) async-start(bf16[4,8,512]{2,1,0:T(8,128)(2,1)} %bitcast.27), calls=%async_computation.4 | async-start | bytes 65536 | tf_op jit(solution)/shard_map/all_to_all | solution.py:124
  56.0 0.2 convolution_convert_fusion
  56.3 0.2 multiply_reduce_fusion
  56.5 0.7 all_to_all.30
  57.2 3.6 %all-to-all-done.4 = bf16[4,8,512]{2,1,0:T(8,128)(2,1)S(1)} async-done(((bf16[4,8,512]{2,1,0:T(8,128)(2,1)}), bf16[4,8,512]{2,1,0:T(8,128)(2,1)S(1)}, u32[]{:S(2)}, u32[]{:S(2)}) %all-to-all-start.4) | async-done | bytes 32800 | tf_op jit(solution)/shard_map/all_to_all | solution.py:124
  60.8 3.4 %all-to-all-start.2 = ((bf16[8,4,2048]{2,1,0:T(4,128)(2,1)}), bf16[8,4,2048]{2,1,0:T(4,128)(2,1)S(1)}, u32[]{:S(2)}, u32[]{:S(2)}) async-start(bf16[8,4,2048]{2,1,0:T(4,128)(2,1)} %all_to_all.30), calls=%async_computation.2 | async-start | bytes 262144 | tf_op jit(solution)/shard_map/all_to_all | solution.py:114
  64.2 6.7 %all-to-all-done.2 = bf16[8,4,2048]{2,1,0:T(4,128)(2,1)S(1)} async-done(((bf16[8,4,2048]{2,1,0:T(4,128)(2,1)}), bf16[8,4,2048]{2,1,0:T(4,128)(2,1)S(1)}, u32[]{:S(2)}, u32[]{:S(2)}) %all-to-all-start.2) | async-done | bytes 131104 | tf_op jit(solution)/shard_map/all_to_all | solution.py:114
  70.8 3.4 %all-to-all-start.5 = ((bf16[8,8,2048]{2,1,0:T(8,128)(2,1)}), bf16[8,8,2048]{2,1,0:T(8,128)(2,1)S(1)}, u32[]{:S(2)}, u32[]{:S(2)}) async-start(bf16[8,8,2048]{2,1,0:T(8,128)(2,1)} %pad_maximum_fusion), calls=%async_computation.5 | async-start | bytes 524288 | tf_op jit(solution)/shard_map/all_to_all | solution.py:24
  74.3 2.3 %fusion.4 = f32[32,640]{1,0:T(8,128)S(1)} fusion(bf16[32,2048]{1,0:T(8,128)(2,1)S(1)} %all_to_all.32, bf16[1,2048,640]{2,1,0:T(8,128)(2,1)} %param.35), kind=kOutput, calls=%fused_computation.4 | convolution fusion | flops 83886080 | bytes 2834432 | tf_op jit(solution)/shard_map/dot_general | solution.py:132
  76.6 2.7 %fusion.6 = bf16[32,2048]{1,0:T(8,128)(2,1)S(1)} fusion(bf16[1,640,2048]{2,1,0:T(8,128)(2,1)S(1)} %copy-done, bf16[32,2048]{1,0:T(8,128)(2,1)S(1)} %all_to_all.32, bf16[1,2048,640]{2,1,0:T(8,128)(2,1)} %param.36, f32[32,640]{1,0:T(8,128)S(1)} %fusion.4), kind=kOutput, calls=%fused_computation.6 | convolution fusion | flops 167960576 | bytes 5586944 | tf_op jit(solution)/shard_map/dot_general | solution.py:135
  79.4 0.7 copy.35
  80.1 3.8 %all-to-all-done.5 = bf16[8,8,2048]{2,1,0:T(8,128)(2,1)S(1)} async-done(((bf16[8,8,2048]{2,1,0:T(8,128)(2,1)}), bf16[8,8,2048]{2,1,0:T(8,128)(2,1)S(1)}, u32[]{:S(2)}, u32[]{:S(2)}) %all-to-all-start.5) | async-done | bytes 262176 | tf_op jit(solution)/shard_map/all_to_all | solution.py:24
  83.9 2.6 %all-to-all-start.3 = ((bf16[32,4,512]{2,1,0:T(4,128)(2,1)}), bf16[32,4,512]{2,1,0:T(4,128)(2,1)S(1)}, u32[]{:S(2)}, u32[]{:S(2)}) async-start(bf16[32,4,512]{2,1,0:T(4,128)(2,1)} %bitcast.24), calls=%async_computation.3 | async-start | bytes 262144 | tf_op jit(solution)/shard_map/all_to_all | solution.py:137
  86.6 0.6 slice.9
  87.2 0.7 fusion.61
  87.9 6.9 %all-to-all-done.3 = bf16[32,4,512]{2,1,0:T(4,128)(2,1)S(1)} async-done(((bf16[32,4,512]{2,1,0:T(4,128)(2,1)}), bf16[32,4,512]{2,1,0:T(4,128)(2,1)S(1)}, u32[]{:S(2)}, u32[]{:S(2)}) %all-to-all-start.3) | async-done | bytes 131104 | tf_op jit(solution)/shard_map/all_to_all | solution.py:137
  94.9 0.2 fusion.20
  95.1 0.7 add_convert_fusion
  (41 shorter events, 1.0 us)
Async XLA Ops:
  0.6 75.9 %copy-start = (bf16[1,640,2048]{2,1,0:T(8,128)(2,1)S(1)}, bf16[1,640,2048]{2,1,0:T(8,128)(2,1)}, u32[]{:S(2)}) copy-start(bf16[1,640,2048]{2,1,0:T(8,128)(2,1)} %param.37) | copy-start | bytes 7864324
  0.6 30.8 %copy-start.7 = (f32[128]{0:T(128)S(1)}, f32[128]{0:T(128)}, u32[]{:S(2)}) copy-start(f32[128]{0:T(128)} %param.26) | copy-start | bytes 1540
  7.3 12.1 %all-to-all-start = ((bf16[8,8,256]{2,1,0:T(8,128)(2,1)}), bf16[8,8,256]{2,1,0:T(8,128)(2,1)S(1)}, u32[]{:S(2)}, u32[]{:S(2)}) async-start(bf16[8,8,256]{2,1,0:T(8,128)(2,1)} %constant_dynamic-update-slice_fusion), calls=%async_computation | async-start | bytes 65536 | tf_op jit(solution)/shard_map/all_to_all | solution.py:12
  21.3 10.1 %all-to-all-start.1 = ((bf16[8,8,1024]{2,1,0:T(8,128)(2,1)}), bf16[8,8,1024]{2,1,0:T(8,128)(2,1)S(1)}, u32[]{:S(2)}, u32[]{:S(2)}) async-start(bf16[8,8,1024]{2,1,0:T(8,128)(2,1)} %fusion.9), calls=%async_computation.1 | async-start | bytes 262144 | tf_op jit(solution)/shard_map/all_to_all | solution.py:24
  31.6 5.8 %copy-start.9 = (f32[8]{0:T(128)S(1)}, f32[8]{0:T(128)}, u32[]{:S(2)}) copy-start(f32[8]{0:T(128)} %param.27) | copy-start | bytes 100
  31.6 6.4 %copy-start.1 = (bf16[8,8,512,128]{3,2,1,0:T(8,128)(2,1)S(1)}, bf16[8,8,512,128]{3,2,1,0:T(8,128)(2,1)}, u32[]{:S(2)}) copy-start(bf16[8,8,512,128]{3,2,1,0:T(8,128)(2,1)} %param.29) | copy-start | bytes 25165828
  37.9 2.2 %copy-start.2 = (bf16[1024,2048]{1,0:T(8,128)(2,1)S(1)}, bf16[1024,2048]{1,0:T(8,128)(2,1)}, u32[]{:S(2)}) copy-start(bf16[1024,2048]{1,0:T(8,128)(2,1)} %param.31) | copy-start | bytes 12582916
  39.1 10.3 %copy-start.4 = (bf16[8,2048]{1,0:T(8,128)(2,1)S(1)}, bf16[8,2048]{1,0:T(8,128)(2,1)}, u32[]{:S(2)}) copy-start(bf16[8,2048]{1,0:T(8,128)(2,1)} %param.21) | copy-start | bytes 98308
  39.1 10.4 %copy-start.3 = (bf16[2048,256]{1,0:T(8,128)(2,1)S(1)}, bf16[2048,256]{1,0:T(8,128)(2,1)}, u32[]{:S(2)}) copy-start(bf16[2048,256]{1,0:T(8,128)(2,1)} %param.38) | copy-start | bytes 3145732
  39.2 10.4 %copy-start.5 = (f32[2048]{0:T(1024)S(1)}, f32[2048]{0:T(1024)}, u32[]{:S(2)}) copy-start(f32[2048]{0:T(1024)} %param.32) | copy-start | bytes 24580
  40.8 15.5 %copy-start.6 = (f32[2048]{0:T(1024)S(1)}, f32[2048]{0:T(1024)}, u32[]{:S(2)}) copy-start(f32[2048]{0:T(1024)} %param.41) | copy-start | bytes 24580
  52.8 8.0 %all-to-all-start.4 = ((bf16[4,8,512]{2,1,0:T(8,128)(2,1)}), bf16[4,8,512]{2,1,0:T(8,128)(2,1)S(1)}, u32[]{:S(2)}, u32[]{:S(2)}) async-start(bf16[4,8,512]{2,1,0:T(8,128)(2,1)} %bitcast.27), calls=%async_computation.4 | async-start | bytes 65536 | tf_op jit(solution)/shard_map/all_to_all | solution.py:124
  60.8 10.1 %all-to-all-start.2 = ((bf16[8,4,2048]{2,1,0:T(4,128)(2,1)}), bf16[8,4,2048]{2,1,0:T(4,128)(2,1)S(1)}, u32[]{:S(2)}, u32[]{:S(2)}) async-start(bf16[8,4,2048]{2,1,0:T(4,128)(2,1)} %all_to_all.30), calls=%async_computation.2 | async-start | bytes 262144 | tf_op jit(solution)/shard_map/all_to_all | solution.py:114
  70.8 13.1 %all-to-all-start.5 = ((bf16[8,8,2048]{2,1,0:T(8,128)(2,1)}), bf16[8,8,2048]{2,1,0:T(8,128)(2,1)S(1)}, u32[]{:S(2)}, u32[]{:S(2)}) async-start(bf16[8,8,2048]{2,1,0:T(8,128)(2,1)} %pad_maximum_fusion), calls=%async_computation.5 | async-start | bytes 524288 | tf_op jit(solution)/shard_map/all_to_all | solution.py:24
  76.6 18.4 %copy-start.8 = (f32[8,2]{0,1:T(2,128)S(1)}, f32[8,2]{0,1:T(2,128)}, u32[]{:S(2)}) copy-start(f32[8,2]{0,1:T(2,128)} %param.34) | copy-start | bytes 196
  83.9 10.9 %all-to-all-start.3 = ((bf16[32,4,512]{2,1,0:T(4,128)(2,1)}), bf16[32,4,512]{2,1,0:T(4,128)(2,1)S(1)}, u32[]{:S(2)}, u32[]{:S(2)}) async-start(bf16[32,4,512]{2,1,0:T(4,128)(2,1)} %bitcast.24), calls=%async_computation.3 | async-start | bytes 262144 | tf_op jit(solution)/shard_map/all_to_all | solution.py:137
